TPU v7x, 128 devices: a 2x2x16 block of a 8x8x16 slice. The times are simulated.
128 devices in a mesh: grp: 4 (over y, x), ep: 32 (over z, core).
Axes of the slice: x: 2, y: 2, z: 16, core: 2. Of those that a mesh axis runs over, the one named last changes fastest.
The devices are a block of a 8x8x16 slice.
Arguments:
- tokens: bfloat16 [2048, 2048], P(('grp', 'ep')), parts along dimension 0, may hold values from -6 to 6
- norm_gain: bfloat16 [2048], replicated, may hold values from 0.099609375 to 1.8984375
- query_weight: bfloat16 [2048, 1024], P(None, 'ep'), may hold values from -0.125 to 0.125
- key_weight: bfloat16 [2048, 256], replicated, may hold values from -0.25 to 0.25
- value_weight: bfloat16 [2048, 256], replicated, may hold values from -0.125 to 0.125
- out_weight: bfloat16 [1024, 2048], P(None, 'ep'), may hold values from -0.1875 to 0.1875
- head_gain: bfloat16 [128], replicated, may hold values from 0.099609375 to 1.8984375
- lambdas: float32 [8], replicated, may hold values from 0.3 to 0.8
- cache_keys: bfloat16 [2048, 1024, 2, 128], P(('grp', 'ep')), parts along dimension 0, may hold values from -1000 to 1000
- cache_values: bfloat16 [2048, 1024, 2, 128], P(('grp', 'ep')), parts along dimension 0, may hold values from -6 to 6
- lengths: int32 [2048], P(('grp', 'ep')), parts along dimension 0, may hold values from 64 to 1024
- moe_gain: bfloat16 [2048], replicated, may hold values from 0.099609375 to 1.8984375
- gate_weight: bfloat16 [32, 2048, 1024], P('ep'), may hold values from -0.375 to 0.375
- up_weight: bfloat16 [32, 2048, 1024], P('ep'), may hold values from -0.375 to 0.375
- down_weight: bfloat16 [32, 1024, 2048], P('ep'), may hold values from -0.02734375 to 0.02734375
- routes: int32 [2048, 4], P(('grp', 'ep')), parts along dimension 0, may hold values from 0 to 31, all different within a row; in each aligned block of 16 rows (0 to 15, 16 to 31, ...) at most 4 rows name the same one
- route_weights: float32 [2048, 4], P(('grp', 'ep')), parts along dimension 0, may hold values from 0.2 to 1
Outputs:
- mixed: bfloat16 [2048, 2048], P(('grp', 'ep')), parts along dimension 0
There are 4 independent parts, one for each index of `grp`. A program takes and returns all parts, laid end to end along the dimension named above; an argument that names none is the same for every part. Nothing has to cross between parts.
Inputs may be any that keep to these rules, and one draw needn't show every extreme that they name: `routes`: a token's 4 experts differ; the tokens of one device name each expert at most 4 times, and in every draw some expert is named exactly 4 times by one device's tokens.
All inputs are finite; a program needn't handle non-finite values.
Results may differ from a plain program's by a relative error of at most 0.034.
Values may be sent and summed in bfloat16 or wider, within the bound.
A program may use at most 128 MiB of HBM per device.

v0:
```python
import jax
import jax.numpy as jnp
from jax import lax
from jax.sharding import Mesh
from jax.sharding import PartitionSpec as P

EP = ("ep_0", "ep_1")
GRP_EP = ("grp", "ep_0", "ep_1")
epsilon = 1e-06
masked_score = -1e30
clamp_limit = 7.0
swish_alpha = 1.702


def in_blocks(value, dim, length):
    before, after = (value.shape[:dim], value.shape[dim + 1 :])
    return jnp.moveaxis(value.reshape(*before, length, -1, *after), dim, 0)


def joined_along(blocks, dim):
    blocks = jnp.moveaxis(blocks, 0, dim)
    lengths = blocks.shape
    return blocks.reshape(*lengths[:dim], lengths[dim] * lengths[dim + 1], *lengths[dim + 2 :])


def moved_by_axis(blocks, axes, sequence):
    inside = blocks.shape[1:]
    filled = blocks.reshape(*(lax.axis_size(a) for a in axes), *inside)
    for k in sequence:
        filled = lax.all_to_all(filled, axes[k], k, k, tiled=True)
    return filled.reshape(-1, *inside)


def two_step_exchange(value, groups, sequence, split_dim, concat_dim):
    length = lax.axis_size(groups[0]) * lax.axis_size(groups[1])
    blocks = in_blocks(value, split_dim, length)
    return joined_along(moved_by_axis(blocks, groups, sequence), concat_dim)


def rms_scaled(values, gain):
    floats = values.astype(jnp.float32)
    return (
        floats
        * lax.rsqrt(jnp.mean(floats * floats, axis=-1, keepdims=True) + epsilon)
        * gain.astype(jnp.float32)
    )


def attention(queries, new_keys, new_values, cache_keys, cache_values, lengths, lambdas, head_gain):
    count = queries.shape[0]
    ctx_len = cache_keys.shape[1]
    kv_count = cache_keys.shape[2]
    head_dim = cache_keys.shape[3] // 2
    heads = lambdas.shape[0]
    group = heads // kv_count
    val_dim = cache_values.shape[3]
    query_grid = queries.reshape(count, kv_count, group, 2, head_dim)
    key_grid = cache_keys.reshape(count, ctx_len, kv_count, 2, head_dim)
    own_keys = new_keys.reshape(count, kv_count, 2, head_dim)
    inv_scale = head_dim ** (-0.5)
    scores = (
        jnp.einsum("bkgcd,bjkcd->bkgcj", query_grid, key_grid, preferred_element_type=jnp.float32)
        * inv_scale
    )
    own_score = (
        jnp.einsum("bkgcd,bkcd->bkgc", query_grid, own_keys, preferred_element_type=jnp.float32)
        * inv_scale
    )
    visible = jnp.arange(ctx_len, dtype=jnp.int32)[None, :] < lengths[:, None]
    scores = jnp.where(visible[:, None, None, None, :], scores, masked_score)
    highest = jnp.maximum(jnp.max(scores, axis=-1), own_score)
    expd = jnp.exp(scores - highest[..., None])
    own_exp = jnp.exp(own_score - highest)
    denominator = jnp.sum(expd, axis=-1) + own_exp
    probs = expd / denominator[..., None]
    own_prob = own_exp / denominator
    lambda_grid = lambdas.reshape(kv_count, group)[None, :, :]
    weights = (probs[:, :, :, 0] - lambda_grid[..., None] * probs[:, :, :, 1]).astype(jnp.bfloat16)
    own_weight = (own_prob[..., 0] - lambda_grid * own_prob[..., 1]).astype(jnp.bfloat16)
    attended = jnp.einsum(
        "bkgj,bjkv->bkgv", weights, cache_values, preferred_element_type=jnp.float32
    )
    own_vals = new_values.reshape(count, kv_count, val_dim).astype(jnp.float32)
    attended = attended + own_weight.astype(jnp.float32)[..., None] * own_vals[:, :, None, :]
    return rms_scaled(attended, head_gain).reshape(count, heads * val_dim).astype(jnp.bfloat16)


def expert_mlp(inputs, gate_w, up_w, down_w):
    gate = jnp.dot(inputs, gate_w, preferred_element_type=jnp.float32)
    upper = jnp.dot(inputs, up_w, preferred_element_type=jnp.float32)
    gate = jnp.minimum(gate, clamp_limit)
    upper = jnp.clip(upper, -clamp_limit, clamp_limit)
    act = ((upper + 1.0) * gate * jax.nn.sigmoid(swish_alpha * gate)).astype(jnp.bfloat16)
    return jnp.dot(act, down_w, preferred_element_type=jnp.float32).astype(jnp.bfloat16)


def local(
    tokens,
    norm_gain,
    query_weight,
    key_weight,
    value_weight,
    out_weight,
    head_gain,
    lambdas,
    cache_keys,
    cache_values,
    lengths,
    moe_gain,
    gate_weight,
    up_weight,
    down_weight,
    routes,
    route_weights,
):
    count = tokens.shape[0]
    width = tokens.shape[1]
    topk = routes.shape[1]
    normed = rms_scaled(tokens, norm_gain).astype(jnp.bfloat16)
    new_keys = jnp.dot(normed, key_weight, preferred_element_type=jnp.float32).astype(jnp.bfloat16)
    new_values = jnp.dot(normed, value_weight, preferred_element_type=jnp.float32).astype(
        jnp.bfloat16
    )
    queries = jnp.dot(
        normed,
        lax.all_gather(query_weight, EP, axis=1, tiled=True),
        preferred_element_type=jnp.float32,
    ).astype(jnp.bfloat16)
    head_out = attention(
        queries, new_keys, new_values, cache_keys, cache_values, lengths, lambdas, head_gain
    )
    attn_out = jnp.dot(
        head_out,
        lax.all_gather(out_weight, EP, axis=1, tiled=True),
        preferred_element_type=jnp.float32,
    ).astype(jnp.bfloat16)
    residual = (tokens.astype(jnp.float32) + attn_out.astype(jnp.float32)).astype(jnp.bfloat16)
    moe_in = rms_scaled(residual, moe_gain).astype(jnp.bfloat16)
    experts = lax.axis_size(EP)
    capacity = min(count, max(2, 2 * count * topk // experts))
    onehot = (routes.reshape(-1)[:, None] == jnp.arange(experts, dtype=jnp.int32)[None, :]).astype(
        jnp.int32
    )
    earlier_all = jnp.cumsum(onehot, axis=0) - onehot
    ranks = jnp.sum(earlier_all * onehot, axis=1).reshape(count, topk)
    slot_id = routes * capacity + ranks
    slot_range = jnp.arange(experts * capacity, dtype=jnp.int32)
    dispatch = jnp.any(slot_id[None, :, :] == slot_range[:, None, None], axis=2).astype(
        jnp.bfloat16
    )
    outgoing = jnp.dot(dispatch, moe_in, preferred_element_type=jnp.float32).astype(jnp.bfloat16)
    outgoing = outgoing.reshape(experts, capacity, width)
    received = lax.all_to_all(outgoing, EP, split_axis=0, concat_axis=0, tiled=True)
    flat_rows = received.reshape(-1, width)
    results = expert_mlp(flat_rows, gate_weight[0], up_weight[0], down_weight[0]).reshape(
        received.shape
    )
    returned = two_step_exchange(results, ("ep_0", "ep_1"), (1, 0), 0, 0)
    picked = returned.reshape(-1, width)[slot_id].astype(jnp.float32)
    moe_sum = jnp.sum(route_weights[:, :, None] * picked, axis=1)
    return (residual.astype(jnp.float32) + moe_sum).astype(jnp.bfloat16)


def solution(mesh):
    torus = Mesh(mesh.devices.reshape(mesh.shape["grp"], 16, 2), ("grp", "ep_0", "ep_1"))
    return jax.shard_map(
        local,
        mesh=torus,
        in_specs=(
            P(GRP_EP, None),
            P(),
            P(None, EP),
            P(),
            P(),
            P(None, EP),
            P(),
            P(),
            P(GRP_EP, None, None, None),
            P(GRP_EP, None, None, None),
            P(GRP_EP),
            P(),
            P(EP, None, None),
            P(EP, None, None),
            P(EP, None, None),
            P(GRP_EP, None),
            P(GRP_EP, None),
        ),
        out_specs=P(GRP_EP, None),
        check_vma=False,
    )
```

profile of v0, /device:TPU:196, one launch (start us, length us, event | category | flops | bytes accessed | tf_op | source)
XLA Modules:
  0.0 256.7 jit_solution(1029286353424995351)
XLA Ops:
  6.6 0.7 all-gather.3.cloned.1.call-update
  7.4 0.7 all-gather.5.cloned.1.call-update
  8.1 0.7 convert_element_type.86
  8.8 1.0 fusion.57
  9.8 1.1 convolution_convert_fusion.4
  11.1 21.2 %copy.77 = bf16[16,1024,2,128]{1,3,2,0:T(8,128)(2,1)} copy(bf16[16,1024,2,128]{3,2,1,0:T(2,128)(2,1)} %param.25) | data formatting | bytes 16777216 | tf_op args[8]
  33.7 51.4 %all-gather.3.cloned.1.call-done = bf16[2048,1024]{0,1:T(8,128)(2,1)} async-done(((bf16[2048,32]{0,1:T(8,128)(2,1)}), bf16[2048,1024]{0,1:T(8,128)(2,1)}) %all-gather.3.cloned.1.call-update) | async-done | bytes 4194320 | tf_op jit(solution)/shard_map/all_gather | solution.py:126
  85.0 3.4 %convolution_convert_fusion.2 = bf16[16,1024]{1,0:T(8,128)(2,1)S(1)} fusion(bf16[2048,1024]{0,1:T(8,128)(2,1)} %all-gather.3.cloned.1.call-done, bf16[16,2048]{1,0:T(8,128)(2,1)S(1)} %copy-done.1, f32[2048]{0:T(1024)S(1)} %convert_element_type.86, f32[16]{0:T(128)S(1)} %add_rsqrt_fusion.2), kind=kOutput, calls=%fused_computation.26 | convolution fusion | flops 67256320 | bytes 4300864 | tf_op jit(solution)/shard_map/dot_general | solution.py:124
  88.9 4.7 %fusion.81 = (f32[16,2,4,2]{2,3,1,0:T(2,128)S(1)}, f32[16,2,4,2,1024]{4,2,3,1,0:T(4,128)S(1)}) fusion(bf16[16,1024,2,2,64]{1,4,3,2,0:T(8,128)(2,1)} %bitcast.96, bf16[16,2,4,2,64]{4,3,2,1,0:T(2,128)(2,1)S(1)} %reshape.79, pred[16,1024]{1,0:T(8,128)(4,1)S(1)} %iota_compare_fusion), kind=kOutput, calls=%fused_computation.91 | convolution fusion | flops 34340608 | bytes 9487360 | tf_op jit(solution)/shard_map/bkgcd,bjkcd->bkgcj/dot_general | solution.py:62
  93.8 0.5 fusion.40
  94.8 0.5 fusion.39
  95.3 5.0 %multiply_reduce_fusion.2 = (f32[16,2,4]{2,1,0:T(2,128)S(1)}, f32[16,2,4,128]{3,2,1,0:T(4,128)S(1)}) fusion(f32[16,2,128]{2,1,0:T(2,128)S(1)} %reshape.86, f32[16,2,4]{2,1,0:T(2,128)S(1)} %copy.85, bf16[16,1024,2,128]{3,2,1,0:T(2,128)(2,1)} %param.26, f32[16,2,4,2,1024]{4,2,3,1,0:T(4,128)S(1)} %fusion.39, f32[2,4]{1,0:T(2,128)S(1)} %mul.149), kind=kOutput, calls=%fused_computation.60 | convolution fusion | flops 34013056 | bytes 9520160 | tf_op jit(solution)/shard_map/bkgj,bjkv->bkgv/dot_general | solution.py:80
  100.6 53.6 %all-gather.5.cloned.1.call-done = bf16[1024,2048]{0,1:T(8,128)(2,1)} async-done(((bf16[1024,64]{0,1:T(8,128)(2,1)}), bf16[1024,2048]{0,1:T(8,128)(2,1)}) %all-gather.5.cloned.1.call-update) | async-done | bytes 4194320 | tf_op jit(solution)/shard_map/all_gather | solution.py:134
  154.3 3.5 %multiply_reduce_fusion.1 = (f32[16]{0:T(128)S(1)}, f32[16,2048]{1,0:T(8,128)S(1)}) fusion(bf16[16,1024]{1,0:T(8,128)(2,1)S(1)} %convert_element_type.97, bf16[1024,2048]{0,1:T(8,128)(2,1)} %all-gather.5.cloned.1.call-done, bf16[16,2048]{1,0:T(8,128)(2,1)S(1)} %copy-done.1), kind=kOutput, calls=%fused_computation.56 | convolution fusion | flops 67370992 | bytes 4423744 | tf_op jit(solution)/shard_map/dot_general | solution.py:132
  158.3 40.2 %all_to_all.15 = bf16[32,4,2048]{2,1,0:T(4,128)(2,1)S(1)} all-to-all(bf16[32,4,2048]{2,1,0:T(4,128)(2,1)S(1)} %reshape.83), channel_id=1, replica_groups=mesh['grp'=4,'ep_0'=16,'ep_1'=2] {'ep_0','ep_1'}, dimensions={0} | all-to-all | bytes 1048576 | tf_op jit(solution)/shard_map/all_to_all | solution.py:153
  198.7 2.9 %fusion.20 = f32[128,1024]{1,0:T(8,128)S(1)} fusion(bf16[128,2048]{1,0:T(8,128)(2,1)S(1)} %reshape.84, bf16[1,2048,1024]{2,1,0:T(8,128)(2,1)} %param.29), kind=kOutput, calls=%fused_computation.20 | convolution fusion | flops 537001984 | bytes 5242880 | tf_op jit(solution)/shard_map/dot_general | solution.py:89
  201.6 4.9 %fusion.8 = bf16[128,2048]{1,0:T(8,128)(2,1)S(1)} fusion(bf16[1,1024,2048]{2,1,0:T(8,128)(2,1)} %param.31, f32[128,1024]{1,0:T(8,128)S(1)} %fusion.20, bf16[128,2048]{1,0:T(8,128)(2,1)S(1)} %reshape.84, bf16[1,2048,1024]{2,1,0:T(8,128)(2,1)} %param.30), kind=kOutput, calls=%fused_computation.9 | convolution fusion | flops 1075183616 | bytes 9961472 | tf_op jit(solution)/shard_map/dot_general | solution.py:94
  206.9 4.2 %all_to_all.16 = bf16[16,2,1,4,2048]{4,3,0,2,1:T(4,128)(2,1)S(1)} all-to-all(bf16[16,2,1,4,2048]{4,3,0,2,1:T(4,128)(2,1)S(1)} %copy.92), channel_id=1, replica_groups=mesh['grp'=4,'ep_0'=16,'ep_1'=2] {'ep_1'}, dimensions={1} | all-to-all | bytes 1048576 | tf_op jit(solution)/shard_map/all_to_all | solution.py:30
  211.1 1.0 copy.93
  212.1 5.5 %all-to-all-start.2 = ((bf16[16,2,1,4,2048]{4,3,1,2,0:T(4,128)(2,1)}), bf16[16,2,1,4,2048]{4,3,1,2,0:T(4,128)(2,1)S(1)}, u32[]{:S(2)}, u32[]{:S(2)}) async-start(bf16[16,2,1,4,2048]{4,3,1,2,0:T(4,128)(2,1)} %copy.93), calls=%async_computation.2 | async-start | bytes 1048576 | tf_op jit(solution)/shard_map/all_to_all | solution.py:30
  217.9 29.9 %all-to-all-done.2 = bf16[16,2,1,4,2048]{4,3,1,2,0:T(4,128)(2,1)S(1)} async-done(((bf16[16,2,1,4,2048]{4,3,1,2,0:T(4,128)(2,1)}), bf16[16,2,1,4,2048]{4,3,1,2,0:T(4,128)(2,1)S(1)}, u32[]{:S(2)}, u32[]{:S(2)}) %all-to-all-start.2) | async-done | bytes 524320 | tf_op jit(solution)/shard_map/all_to_all | solution.py:30
  247.9 0.7 gather_fusion
  248.8 0.4 multiply_reduce_fusion
  249.2 0.6 add_convert_fusion
  (64 shorter events, 4.4 us)
Async XLA Ops:
  6.5 3.2 %copy-start = (bf16[2048,256]{1,0:T(8,128)(2,1)S(1)}, bf16[2048,256]{1,0:T(8,128)(2,1)}, u32[]{:S(2)}) copy-start(bf16[2048,256]{1,0:T(8,128)(2,1)} %param.20) | copy-start | bytes 3145732
  6.6 78.5 %all-gather.3.cloned.1.call-start = ((), (), s32[]{:S(2)}) async-start(), calls=%async_computation.3 | async-start | bytes 4325376 | tf_op jit(solution)/shard_map/all_gather | solution.py:126
  7.3 147.0 %all-gather.5.cloned.1.call-start = ((), (), s32[]{:S(2)}) async-start(), calls=%async_computation.4 | async-start | bytes 4325376 | tf_op jit(solution)/shard_map/all_gather | solution.py:134
  11.0 21.3 %copy-start.7 = (f32[8]{0:T(128)S(1)}, f32[8]{0:T(128)}, u32[]{:S(2)}) copy-start(f32[8]{0:T(128)} %param.24) | copy-start | bytes 100
  11.0 21.4 %copy-start.1 = (bf16[16,2048]{1,0:T(8,128)(2,1)S(1)}, bf16[16,2048]{1,0:T(8,128)(2,1)}, u32[]{:S(2)}) copy-start(bf16[16,2048]{1,0:T(8,128)(2,1)} %param.17) | copy-start | bytes 196612
  11.0 21.4 %copy-start.2 = (bf16[2048,256]{1,0:T(8,128)(2,1)S(1)}, bf16[2048,256]{1,0:T(8,128)(2,1)}, u32[]{:S(2)}) copy-start(bf16[2048,256]{1,0:T(8,128)(2,1)} %param.21) | copy-start | bytes 3145732
  11.0 21.7 %copy-start.8 = (bf16[128]{0:T(256)(128)(2,1)S(1)}, bf16[128]{0:T(256)(128)(2,1)}, u32[]{:S(2)}) copy-start(bf16[128]{0:T(256)(128)(2,1)} %param.23) | copy-start | bytes 772
  11.1 21.7 %copy-start.4 = (s32[16,4]{0,1:T(4,128)S(1)}, s32[16,4]{0,1:T(4,128)}, u32[]{:S(2)}) copy-start(s32[16,4]{0,1:T(4,128)} %param.32) | copy-start | bytes 772
  11.1 22.4 %copy-start.3 = (bf16[2048]{0:T(1024)(128)(2,1)S(1)}, bf16[2048]{0:T(1024)(128)(2,1)}, u32[]{:S(2)}) copy-start(bf16[2048]{0:T(1024)(128)(2,1)} %param.28) | copy-start | bytes 12292
  11.1 22.5 %copy-start.6 = (s32[16]{0:T(128)S(1)}, s32[16]{0:T(128)}, u32[]{:S(2)}) copy-start(s32[16]{0:T(128)} %param.27) | copy-start | bytes 196
  206.5 11.3 %copy-start.5 = (f32[16,4]{0,1:T(4,128)S(1)}, f32[16,4]{0,1:T(4,128)}, u32[]{:S(2)}) copy-start(f32[16,4]{0,1:T(4,128)} %param.33) | copy-start | bytes 772
  212.1 35.6 %all-to-all-start.2 = ((bf16[16,2,1,4,2048]{4,3,1,2,0:T(4,128)(2,1)}), bf16[16,2,1,4,2048]{4,3,1,2,0:T(4,128)(2,1)S(1)}, u32[]{:S(2)}, u32[]{:S(2)}) async-start(bf16[16,2,1,4,2048]{4,3,1,2,0:T(4,128)(2,1)} %copy.93), calls=%async_computation.2 | async-start | bytes 1048576 | tf_op jit(solution)/shard_map/all_to_all | solution.py:30
Sparse Core Ops, SparseCore 0:
  9.1 75.9 all-gather.2
  86.7 67.4 all-gather.4
where the time goes:
time: 258 us; the launch traced here: 257 us
  waiting for transfers between devices  136 us (53%)
  blocking collectives  44.4 us (17%)
  matrix products  26.3 us (10%)
  local copies, waits for them, and re-layouts  25.8 us (10%)
  between operations  13.7 us (5%)
  starting transfers between devices  5.6 us (2%)
  other arithmetic  4.51 us (2%)
    all_gather x1, waiting for transfers between devices, local(): lax.all_gather(out_weight, EP, axis=1, tiled=True)  53.6 us
    all_gather x1, waiting for transfers between devices, local(): lax.all_gather(query_weight, EP, axis=1, tiled=True)  51.4 us
    all_to_all x1, blocking collectives, local(): lax.all_to_all(outgoing, EP, split_axis=0, concat_axis=0, tiled=True)  40.2 us
    all_to_all x1, waiting for transfers between devices, moved_by_axis(): filled = lax.all_to_all(filled, axes[k], k, k, tiled=True)  29.9 us
    unnamed x21, local copies, waits for them, and re-layouts  21.5 us
    all_to_all x1, starting transfers between devices, moved_by_axis(): filled = lax.all_to_all(filled, axes[k], k, k, tiled=True)  5.54 us
  transfers between devices with their start and end apart: 3, of which 3 were waited for; matrix products, arithmetic and copies ran while one was open for 16% of the time, Pallas kernels for 0%

commit v1 on v0

--- a/solution.py
+++ b/solution.py
@@ -123,7 +123,9 @@
     )
     queries = jnp.dot(
         normed,
-        lax.all_gather(query_weight, EP, axis=1, tiled=True),
+        jnp.concatenate(
+            lax.all_to_all(jnp.stack([query_weight] * lax.axis_size(EP)), EP, 0, 0), axis=1
+        ),
         preferred_element_type=jnp.float32,
     ).astype(jnp.bfloat16)
     head_out = attention(

time: 258 us -> 352 us (1.36)
  waiting for transfers between devices: 136 us -> 217 us
  starting transfers between devices: 5.6 us -> 22.7 us
  blocking collectives: 44.4 us -> 40.5 us
    all_to_all x0 -> x1, waiting for transfers between devices: none -> 186 us  [local(): lax.all_to_all(jnp.stack([query_weight] * lax.axis_size(EP)), EP, 0, 0)]
    all_gather x1, waiting for transfers between devices: 53.6 us -> 0.02 us  [local(): lax.all_gather(out_weight, EP, axis=1, tiled=True)]
    all_gather x1 -> x0, waiting for transfers between devices: 51.4 us -> none  [local(): lax.all_gather(query_weight, EP, axis=1, tiled=True)]
    all_to_all x0 -> x1, starting transfers between devices: none -> 17.1 us  [local(): lax.all_to_all(jnp.stack([query_weight] * lax.axis_size(EP)), EP, 0, 0)]
    all_to_all x1, blocking collectives: 40.2 us -> 36.4 us  [local(): lax.all_to_all(outgoing, EP, split_axis=0, concat_axis=0, tiled=True)]
    unnamed x21 -> x23, local copies, waits for them, and re-layouts: 21.5 us -> 21.5 us
  transfers between devices with their start and end apart: 3 -> 3, of which waited for: 3 -> 2; matrix products, arithmetic and copies ran while one was open for 16% -> 11% of each run, Pallas kernels for 0% -> 0%
where the time goes in v1:
time: 352 us; the launch traced here: 351 us
  waiting for transfers between devices  217 us (62%)
  blocking collectives  40.5 us (12%)
  local copies, waits for them, and re-layouts  29.2 us (8%)
  matrix products  25.4 us (7%)
  starting transfers between devices  22.7 us (6%)
  between operations  13.7 us (4%)
    all_to_all x1, waiting for transfers between devices, local(): lax.all_to_all(jnp.stack([query_weight] * lax.axis_size(EP)), EP, 0, 0)  186 us
    all_to_all x1, blocking collectives, local(): lax.all_to_all(outgoing, EP, split_axis=0, concat_axis=0, tiled=True)  36.4 us
    all_to_all x1, waiting for transfers between devices, moved_by_axis(): filled = lax.all_to_all(filled, axes[k], k, k, tiled=True)  29.9 us
    unnamed x23, local copies, waits for them, and re-layouts  21.5 us
    all_to_all x1, starting transfers between devices, local(): lax.all_to_all(jnp.stack([query_weight] * lax.axis_size(EP)), EP, 0, 0)  17.1 us
  transfers between devices with their start and end apart: 3, of which 2 were waited for; matrix products, arithmetic and copies ran while one was open for 11% of the time, Pallas kernels for 0%

profile of v1, /device:TPU:196, one launch (start us, length us, event | category | flops | bytes accessed | tf_op | source)
XLA Modules:
  0.0 351.2 jit_solution(16886126520471001034)
XLA Ops:
  6.6 3.4 stack.2
  10.0 17.1 %all-to-all-start = ((bf16[32,2048,32]{1,2,0:T(8,128)(2,1)}), bf16[32,2048,32]{1,2,0:T(8,128)(2,1)}, u32[]{:S(2)}, u32[]{:S(2)}) async-start(bf16[32,2048,32]{1,2,0:T(8,128)(2,1)} %stack.2), calls=%async_computation | async-start | bytes 8388608 | tf_op jit(solution)/shard_map/all_to_all | solution.py:127
  27.2 0.7 all-gather.2.cloned.1.call-update
  28.1 0.3 convolution_convert_fusion.4
  28.6 21.3 %copy.78 = bf16[16,1024,2,128]{1,3,2,0:T(8,128)(2,1)} copy(bf16[16,1024,2,128]{3,2,1,0:T(2,128)(2,1)} %param.25) | data formatting | bytes 16777216 | tf_op args[8]
  49.9 0.3 fusion.38
  51.2 186.0 %all-to-all-done = bf16[32,2048,32]{1,2,0:T(8,128)(2,1)} async-done(((bf16[32,2048,32]{1,2,0:T(8,128)(2,1)}), bf16[32,2048,32]{1,2,0:T(8,128)(2,1)}, u32[]{:S(2)}, u32[]{:S(2)}) %all-to-all-start) | async-done | bytes 4194336 | tf_op jit(solution)/shard_map/all_to_all | solution.py:127
  237.2 3.4 convolution_convert_fusion.2
  241.0 4.7 %fusion.81 = (f32[16,2,4,2]{2,3,1,0:T(2,128)S(1)}, f32[16,2,4,2,1024]{4,2,3,1,0:T(4,128)S(1)}) fusion(bf16[16,1024,2,2,64]{1,4,3,2,0:T(8,128)(2,1)} %bitcast.99, bf16[16,2,4,2,64]{4,3,2,1,0:T(2,128)(2,1)S(1)} %reshape.89, pred[16,1024]{1,0:T(8,128)(4,1)S(1)} %iota_compare_fusion), kind=kOutput, calls=%fused_computation.91 | convolution fusion | flops 34340608 | bytes 9487360 | tf_op jit(solution)/shard_map/bkgcd,bjkcd->bkgcj/dot_general | solution.py:62
  245.9 0.5 fusion.40
  246.9 0.5 fusion.39
  247.4 4.9 %multiply_reduce_fusion.2 = (f32[16,2,4]{2,1,0:T(2,128)S(1)}, f32[16,2,4,128]{3,2,1,0:T(4,128)S(1)}) fusion(f32[16,2,128]{2,1,0:T(2,128)S(1)} %reshape.96, f32[16,2,4]{2,1,0:T(2,128)S(1)} %copy.86, bf16[16,1024,2,128]{3,2,1,0:T(2,128)(2,1)} %param.26, f32[16,2,4,2,1024]{4,2,3,1,0:T(4,128)S(1)} %fusion.39, f32[2,4]{1,0:T(2,128)S(1)} %mul.149), kind=kOutput, calls=%fused_computation.60 | convolution fusion | flops 34013056 | bytes 9520160 | tf_op jit(solution)/shard_map/bkgj,bjkv->bkgv/dot_general | solution.py:80
  252.7 3.5 multiply_reduce_fusion.1
  256.2 0.4 convolution_convert_fusion
  256.7 36.4 %all_to_all.20 = bf16[32,4,2048]{2,1,0:T(4,128)(2,1)S(1)} all-to-all(bf16[32,4,2048]{2,1,0:T(4,128)(2,1)S(1)} %reshape.93), channel_id=1, replica_groups=mesh['grp'=4,'ep_0'=16,'ep_1'=2] {'ep_0','ep_1'}, dimensions={0} | all-to-all | bytes 1048576 | tf_op jit(solution)/shard_map/all_to_all | solution.py:155
  293.2 2.9 fusion.20
  296.2 4.9 %fusion.8 = bf16[128,2048]{1,0:T(8,128)(2,1)S(1)} fusion(bf16[1,1024,2048]{2,1,0:T(8,128)(2,1)} %param.31, f32[128,1024]{1,0:T(8,128)S(1)} %fusion.20, bf16[128,2048]{1,0:T(8,128)(2,1)S(1)} %reshape.94, bf16[1,2048,1024]{2,1,0:T(8,128)(2,1)} %param.30), kind=kOutput, calls=%fused_computation.9 | convolution fusion | flops 1075183616 | bytes 9961472 | tf_op jit(solution)/shard_map/dot_general | solution.py:94
  301.5 4.2 %all_to_all.21 = bf16[16,2,1,4,2048]{4,3,0,2,1:T(4,128)(2,1)S(1)} all-to-all(bf16[16,2,1,4,2048]{4,3,0,2,1:T(4,128)(2,1)S(1)} %copy.93), channel_id=1, replica_groups=mesh['grp'=4,'ep_0'=16,'ep_1'=2] {'ep_1'}, dimensions={1} | all-to-all | bytes 1048576 | tf_op jit(solution)/shard_map/all_to_all | solution.py:30
  305.7 1.0 copy.94
  306.7 5.5 %all-to-all-start.3 = ((bf16[16,2,1,4,2048]{4,3,1,2,0:T(4,128)(2,1)}), bf16[16,2,1,4,2048]{4,3,1,2,0:T(4,128)(2,1)S(1)}, u32[]{:S(2)}, u32[]{:S(2)}) async-start(bf16[16,2,1,4,2048]{4,3,1,2,0:T(4,128)(2,1)} %copy.94), calls=%async_computation.3 | async-start | bytes 1048576 | tf_op jit(solution)/shard_map/all_to_all | solution.py:30
  312.4 29.9 %all-to-all-done.3 = bf16[16,2,1,4,2048]{4,3,1,2,0:T(4,128)(2,1)S(1)} async-done(((bf16[16,2,1,4,2048]{4,3,1,2,0:T(4,128)(2,1)}), bf16[16,2,1,4,2048]{4,3,1,2,0:T(4,128)(2,1)S(1)}, u32[]{:S(2)}, u32[]{:S(2)}) %all-to-all-start.3) | async-done | bytes 524320 | tf_op jit(solution)/shard_map/all_to_all | solution.py:30
  342.4 0.7 gather_fusion
  343.3 0.4 multiply_reduce_fusion
  343.7 0.6 add_convert_fusion
  (66 shorter events, 3.9 us)
Async XLA Ops:
  6.5 21.6 %copy-start = (bf16[2048,256]{1,0:T(8,128)(2,1)S(1)}, bf16[2048,256]{1,0:T(8,128)(2,1)}, u32[]{:S(2)}) copy-start(bf16[2048,256]{1,0:T(8,128)(2,1)} %param.20) | copy-start | bytes 3145732
  10.0 18.0 %copy-start.3 = (bf16[2048]{0:T(1024)(128)(2,1)S(1)}, bf16[2048]{0:T(1024)(128)(2,1)}, u32[]{:S(2)}) copy-start(bf16[2048]{0:T(1024)(128)(2,1)} %param.18) | copy-start | bytes 12292
  10.0 18.0 %copy-start.1 = (bf16[16,2048]{1,0:T(8,128)(2,1)S(1)}, bf16[16,2048]{1,0:T(8,128)(2,1)}, u32[]{:S(2)}) copy-start(bf16[16,2048]{1,0:T(8,128)(2,1)} %param.17) | copy-start | bytes 196612
  10.0 227.2 %all-to-all-start = ((bf16[32,2048,32]{1,2,0:T(8,128)(2,1)}), bf16[32,2048,32]{1,2,0:T(8,128)(2,1)}, u32[]{:S(2)}, u32[]{:S(2)}) async-start(bf16[32,2048,32]{1,2,0:T(8,128)(2,1)} %stack.2), calls=%async_computation | async-start | bytes 8388608 | tf_op jit(solution)/shard_map/all_to_all | solution.py:127
  27.1 225.5 %all-gather.2.cloned.1.call-start = ((), (), s32[]{:S(2)}) async-start(), calls=%async_computation.4 | async-start | bytes 4325376 | tf_op jit(solution)/shard_map/all_gather | solution.py:136
  28.5 21.3 %copy-start.8 = (f32[8]{0:T(128)S(1)}, f32[8]{0:T(128)}, u32[]{:S(2)}) copy-start(f32[8]{0:T(128)} %param.24) | copy-start | bytes 100
  28.5 21.4 %copy-start.2 = (bf16[2048,256]{1,0:T(8,128)(2,1)S(1)}, bf16[2048,256]{1,0:T(8,128)(2,1)}, u32[]{:S(2)}) copy-start(bf16[2048,256]{1,0:T(8,128)(2,1)} %param.21) | copy-start | bytes 3145732
  28.5 21.7 %copy-start.9 = (bf16[128]{0:T(256)(128)(2,1)S(1)}, bf16[128]{0:T(256)(128)(2,1)}, u32[]{:S(2)}) copy-start(bf16[128]{0:T(256)(128)(2,1)} %param.23) | copy-start | bytes 772
  28.5 21.7 %copy-start.5 = (s32[16,4]{0,1:T(4,128)S(1)}, s32[16,4]{0,1:T(4,128)}, u32[]{:S(2)}) copy-start(s32[16,4]{0,1:T(4,128)} %param.32) | copy-start | bytes 772
  28.5 22.4 %copy-start.4 = (bf16[2048]{0:T(1024)(128)(2,1)S(1)}, bf16[2048]{0:T(1024)(128)(2,1)}, u32[]{:S(2)}) copy-start(bf16[2048]{0:T(1024)(128)(2,1)} %param.28) | copy-start | bytes 12292
  28.6 22.5 %copy-start.7 = (s32[16]{0:T(128)S(1)}, s32[16]{0:T(128)}, u32[]{:S(2)}) copy-start(s32[16]{0:T(128)} %param.27) | copy-start | bytes 196
  301.0 11.3 %copy-start.6 = (f32[16,4]{0,1:T(4,128)S(1)}, f32[16,4]{0,1:T(4,128)}, u32[]{:S(2)}) copy-start(f32[16,4]{0,1:T(4,128)} %param.33) | copy-start | bytes 772
  306.7 35.6 %all-to-all-start.3 = ((bf16[16,2,1,4,2048]{4,3,1,2,0:T(4,128)(2,1)}), bf16[16,2,1,4,2048]{4,3,1,2,0:T(4,128)(2,1)S(1)}, u32[]{:S(2)}, u32[]{:S(2)}) async-start(bf16[16,2,1,4,2048]{4,3,1,2,0:T(4,128)(2,1)} %copy.94), calls=%async_computation.3 | async-start | bytes 1048576 | tf_op jit(solution)/shard_map/all_to_all | solution.py:30
Sparse Core Ops, SparseCore 0:
  29.7 142.2 all-gather.1
